TPU v7x, 32 devices: a whole 2x2x4 slice. The times are simulated.
32 devices in a mesh: fs: 16 (over z, y, x), tp: 2 (over core).
Axes of the slice: x: 2, y: 2, z: 4, core: 2. Of those that a mesh axis runs over, the one named last changes fastest.
Arguments:
- normed: bfloat16 [16384, 2048], P('fs'), may hold values from -6 to 6
- key_cot: bfloat16 [16384, 1024], P('fs', 'tp'), may hold values from -130 to 130
- value_cot: bfloat16 [16384, 2048], P('fs', 'tp'), may hold values from -130 to 130
- basis: bfloat16 [2048, 256], P('fs'), may hold values from -3.535534 to 3.535534
- master_key: float32 [2048, 1024], P('fs', 'tp'), may hold values from -3 to 3
- master_value: float32 [2048, 2048], P('fs', 'tp'), may hold values from -3 to 3
- first_key: float32 [256, 1024], P('fs', 'tp'), may hold values from -3 to 3
- second_key: float32 [256, 1024], P('fs', 'tp'), may hold values from 0.05 to 2
- first_value: float32 [256, 2048], P('fs', 'tp'), may hold values from -3 to 3
- second_value: float32 [256, 2048], P('fs', 'tp'), may hold values from 0.05 to 2
Outputs:
- step_key: float32 [2048, 1024], P('fs', 'tp')
- step_value: float32 [2048, 2048], P('fs', 'tp')
- new_master_key: float32 [2048, 1024], P('fs', 'tp')
- new_master_value: float32 [2048, 2048], P('fs', 'tp')
- copy_key: bfloat16 [2048, 1024], P(None, 'tp')
- copy_value: bfloat16 [2048, 2048], P(None, 'tp')
- new_first_key: float32 [256, 1024], P('fs', 'tp')
- new_second_key: float32 [256, 1024], P('fs', 'tp')
- new_first_value: float32 [256, 2048], P('fs', 'tp')
- new_second_value: float32 [256, 2048], P('fs', 'tp')
All inputs are finite; a program needn't handle non-finite values.
Results may differ from a plain program's by a relative error of at most 0.0055.
Values may be sent and summed in bfloat16 or wider, within the bound.
A program may use at most 64 MiB of HBM per device.

v0:
```python
import jax
import jax.numpy as jnp
from jax import lax
from jax.sharding import PartitionSpec as P

DK = 1024
DV = 2048
R = 256
learn_rate = 0.05
beta_first = 0.9
beta_second = 0.9
epsilon = 1e-08
norm_eps = 1e-06


def on_device(
    normed,
    key_cot,
    value_cot,
    basis,
    master_key,
    master_value,
    first_key,
    second_key,
    first_value,
    second_value,
):
    key_cols = key_cot.shape[1]
    cotangents = jnp.concatenate([key_cot, value_cot], axis=1)
    projected = jnp.dot(
        normed, lax.all_gather(basis, "fs", axis=0, tiled=True), preferred_element_type=jnp.float32
    )
    upper_part = projected.astype(jnp.bfloat16)
    lower_part = (projected - upper_part.astype(jnp.float32)).astype(jnp.bfloat16)
    partial_value = lax.dot_general(
        upper_part, cotangents, (((0,), (0,)), ((), ())), preferred_element_type=jnp.float32
    )
    partial_value = partial_value + lax.dot_general(
        lower_part, cotangents, (((0,), (0,)), ((), ())), preferred_element_type=jnp.float32
    )
    rank_rows = first_key.shape[0]
    summed = lax.psum(partial_value, "fs")
    squares = lax.psum(jnp.sum(summed * summed), "tp")
    own_rows = lax.dynamic_slice_in_dim(summed, lax.axis_index("fs") * rank_rows, rank_rows, 0)
    root_mean = jnp.sqrt(squares / (R * (DK + DV)) + norm_eps)
    grad_scale = 1.0 / root_mean
    first_moment = jnp.concatenate([first_key, first_value], axis=1)
    second_moment = jnp.concatenate([second_key, second_value], axis=1)
    scaled = own_rows * grad_scale
    new_first = beta_first * first_moment + (1.0 - beta_first) * scaled
    new_second = beta_second * second_moment + (1.0 - beta_second) * scaled * scaled
    direction = (new_first / (jnp.sqrt(new_second) + epsilon)).astype(jnp.bfloat16)
    all_directions = lax.all_gather(direction, "fs", axis=0, tiled=True)
    update_step = jnp.dot(basis, all_directions, preferred_element_type=jnp.float32)
    master = jnp.concatenate([master_key, master_value], axis=1)
    new_master = master - learn_rate * update_step
    half_copy = new_master.astype(jnp.bfloat16)
    copy_key, copy_value = (
        lax.all_gather(half_copy[:, :key_cols], "fs", axis=0, tiled=True),
        lax.all_gather(half_copy[:, key_cols:], "fs", axis=0, tiled=True),
    )
    return (
        update_step[:, :key_cols],
        update_step[:, key_cols:],
        new_master[:, :key_cols],
        new_master[:, key_cols:],
        copy_key,
        copy_value,
        new_first[:, :key_cols],
        new_second[:, :key_cols],
        new_first[:, key_cols:],
        new_second[:, key_cols:],
    )


def solution(mesh):
    placed = (
        P("fs", None),
        P("fs", "tp"),
        P("fs", "tp"),
        P("fs", None),
        P("fs", "tp"),
        P("fs", "tp"),
        P("fs", "tp"),
        P("fs", "tp"),
        P("fs", "tp"),
        P("fs", "tp"),
    )
    return jax.shard_map(
        on_device,
        mesh=mesh,
        in_specs=placed,
        out_specs=(
            P("fs", "tp"),
            P("fs", "tp"),
            P("fs", "tp"),
            P("fs", "tp"),
            P(None, "tp"),
            P(None, "tp"),
            P("fs", "tp"),
            P("fs", "tp"),
            P("fs", "tp"),
            P("fs", "tp"),
        ),
        check_vma=False,
    )
```

profile of v0, /device:TPU:0, one launch (start us, length us, event | category | flops | bytes accessed | tf_op | source)
XLA Modules:
  0.0 406.0 jit_solution(744935510458757411)
XLA Ops:
  7.2 0.0 all-gather.4.cloned.1.call-start
  7.2 0.7 all-gather.4.cloned.1.call-update
  7.9 0.0 all-reduce.2.cloned.1.call-start
  8.0 0.0 copy-start
  8.0 1.4 constant_dynamic-update-slice_fusion.1
  9.4 0.5 copy-done
  9.9 0.2 constant_dynamic-update-slice_fusion
  10.0 58.5 %all-gather.4.cloned.1.call-done = bf16[2048,256]{1,0:T(8,128)(2,1)} async-done(((bf16[128,256]{1,0:T(8,128)(2,1)}), bf16[2048,256]{1,0:T(8,128)(2,1)}) %all-gather.4.cloned.1.call-update) | async-done | bytes 1048592 | tf_op jit(solution)/shard_map/all_gather | solution.py:31
  68.6 3.7 fusion.6
  72.3 1.0 fusion.1
  73.4 0.0 copy-start.2
  73.4 2.2 convolution_add_fusion
  75.5 0.0 copy-start.3
  75.5 0.0 copy-start.4
  75.5 0.0 copy-start.1
  75.6 0.0 all-reduce.2.cloned.1.call-update
  75.6 0.0 all-gather.6.cloned.1.call-start
  75.6 0.0 copy-done.2
  75.7 0.1 copy.20
  75.8 1.2 copy.21
  77.0 115.1 %all-reduce.2.cloned.1.call-done = f32[256,1536]{1,0:T(8,128)} async-done(((f32[256,1536]{1,0:T(8,128)}), f32[256,1536]{1,0:T(8,128)}) %all-reduce.2.cloned.1.call-update) | async-done | bytes 1572880 | tf_op jit(solution)/shard_map/psum | solution.py:42
  192.1 2.4 multiply_reduce_fusion
  194.5 3.1 psum.15
  198.3 0.0 copy-done.3
  198.3 0.0 copy-done.4
  198.3 0.0 copy-done.5
  198.3 0.0 copy-done.6
  198.3 1.0 divide_convert_fusion
  199.3 43.7 %all_gather.13 = bf16[256,1536]{1,0:T(8,128)(2,1)S(1)} all-gather(bf16[16,1536]{1,0:T(8,128)(2,1)S(1)} %get-tuple-element.22), channel_id=1, replica_groups=mesh['fs'=16,'tp'=2] {'fs'}, dimensions={0}, use_global_device_ids=true | all-gather | bytes 835584 | tf_op jit(solution)/shard_map/all_gather | solution.py:53
  243.0 0.0 copy-done.1
  243.0 0.4 fusion.4
  243.4 0.7 slice.44
  244.1 0.0 all-gather.6.cloned.1.call-update
  244.1 0.0 all-gather.8.cloned.1.call-start
  244.1 0.7 slice.45
  244.9 0.0 all-gather.8.cloned.1.call-update
  244.9 0.6 slice.47
  245.5 0.6 slice.49
  246.1 0.6 slice.46
  246.7 0.6 slice.48
  247.5 1.0 copy.25
  248.5 0.8 copy.24
  249.4 1.0 copy.23
  250.3 0.8 copy.22
  251.2 51.9 %all-gather.6.cloned.1.call-done = bf16[2048,512]{0,1:T(8,128)(2,1)} async-done(((bf16[128,512]{0,1:T(8,128)(2,1)}), bf16[2048,512]{0,1:T(8,128)(2,1)}) %all-gather.6.cloned.1.call-update) | async-done | bytes 2097168 | tf_op jit(solution)/shard_map/all_gather | solution.py:59
  303.0 3.9 copy.26
  307.0 86.1 %all-gather.8.cloned.1.call-done = bf16[2048,1024]{0,1:T(8,128)(2,1)} async-done(((bf16[128,1024]{0,1:T(8,128)(2,1)}), bf16[2048,1024]{0,1:T(8,128)(2,1)}) %all-gather.8.cloned.1.call-update) | async-done | bytes 4194320 | tf_op jit(solution)/shard_map/all_gather | solution.py:60
  393.1 6.4 %copy.27 = bf16[2048,1024]{1,0:T(8,128)(2,1)} copy(bf16[2048,1024]{0,1:T(8,128)(2,1)} %all-gather.8.cloned.1.call-done) | data formatting | bytes 8388608
  (6 shorter events, 0.1 us)
Async XLA Ops:
  7.2 61.4 %all-gather.4.cloned.1.call-start = ((), (), s32[]{:S(2)}) async-start(), calls=%async_computation | async-start | bytes 1114112 | tf_op jit(solution)/shard_map/all_gather | solution.py:31
  7.9 184.2 %all-reduce.2.cloned.1.call-start = ((), (), s32[]{:S(2)}) async-start(), calls=%async_computation.1 | async-start | bytes 3145728 | tf_op jit(solution)/shard_map/psum | solution.py:42
  8.0 1.9 copy-start
  73.4 2.3 copy-start.2
  75.5 122.7 %copy-start.3 = (f32[16,1024]{1,0:T(8,128)S(1)}, f32[16,1024]{1,0:T(8,128)}, u32[]{:S(2)}) copy-start(f32[16,1024]{1,0:T(8,128)} %param.19) | copy-start | bytes 196612
  75.5 122.8 %copy-start.4 = (f32[16,1024]{1,0:T(8,128)S(1)}, f32[16,1024]{1,0:T(8,128)}, u32[]{:S(2)}) copy-start(f32[16,1024]{1,0:T(8,128)} %param.18) | copy-start | bytes 196612
  75.5 122.8 %copy-start.5 = (f32[16,512]{1,0:T(8,128)S(1)}, f32[16,512]{1,0:T(8,128)}, u32[]{:S(2)}) copy-start(f32[16,512]{1,0:T(8,128)} %param.17) | copy-start | bytes 98308
  75.5 122.8 %copy-start.6 = (f32[16,512]{1,0:T(8,128)S(1)}, f32[16,512]{1,0:T(8,128)}, u32[]{:S(2)}) copy-start(f32[16,512]{1,0:T(8,128)} %param.16) | copy-start | bytes 98308
  75.5 167.4 %copy-start.1 = (bf16[128,256]{1,0:T(8,128)(2,1)S(1)}, bf16[128,256]{1,0:T(8,128)(2,1)}, u32[]{:S(2)}) copy-start(bf16[128,256]{1,0:T(8,128)(2,1)} %param.13) | copy-start | bytes 196612
  75.6 227.5 %all-gather.6.cloned.1.call-start = ((), (), s32[]{:S(2)}) async-start(), calls=%async_computation.2 | async-start | bytes 2228224 | tf_op jit(solution)/shard_map/all_gather | solution.py:59
  244.1 149.0 %all-gather.8.cloned.1.call-start = ((), (), s32[]{:S(2)}) async-start(), calls=%async_computation.3 | async-start | bytes 4456448 | tf_op jit(solution)/shard_map/all_gather | solution.py:60
Sparse Core Ops, SparseCore 0:
  10.7 57.7 all-gather.3
  75.7 116.3 all-reduce.1
  244.2 58.7 all-gather.5
  306.2 86.8 all-gather.7
where the time goes:
time: 406 us
  waiting for transfers between devices  312 us (77%)
  blocking collectives  46.8 us (12%)
  local copies, waits for them, and re-layouts  21.4 us (5%)
  between operations  14.6 us (4%)
  matrix products  7.34 us (2%)
    psum x1, waiting for transfers between devices, on_device(): summed = lax.psum(partial_value, 'fs')  115 us
    all_gather x1, waiting for transfers between devices, on_device(): lax.all_gather(half_copy[:, key_cols:], 'fs', axis=0, tiled=True)  86.1 us
    all_gather x1, waiting for transfers between devices, on_device(): lax.all_gather(basis, 'fs', axis=0, tiled=True)  58.5 us
    all_gather x1, waiting for transfers between devices, on_device(): lax.all_gather(half_copy[:, :key_cols], 'fs', axis=0, tiled=True)  51.9 us
    all_gather x1, blocking collectives, on_device(): all_directions = lax.all_gather(direction, 'fs', axis=0, tiled=True)  43.7 us
    unnamed x23, local copies, waits for them, and re-layouts  17.3 us
  transfers between devices with their start and end apart: 4, of which 4 were waited for; matrix products, arithmetic and copies ran while one was open for 3% of the time, Pallas kernels for 0%

commit v1 on v0

--- a/solution.py
+++ b/solution.py
@@ -39,7 +39,8 @@
         lower_part, cotangents, (((0,), (0,)), ((), ())), preferred_element_type=jnp.float32
     )
     rank_rows = first_key.shape[0]
-    summed = lax.psum(partial_value, "fs")
+    pieces = lax.all_gather(partial_value, "fs")
+    summed = jnp.sum(pieces, axis=0)
     squares = lax.psum(jnp.sum(summed * summed), "tp")
     own_rows = lax.dynamic_slice_in_dim(summed, lax.axis_index("fs") * rank_rows, rank_rows, 0)
     root_mean = jnp.sqrt(squares / (R * (DK + DV)) + norm_eps)

time: 406 us -> 566 us (1.39)
  waiting for transfers between devices: 312 us -> 466 us
  other arithmetic: 3.39 us -> 11 us
    all_gather x0 -> x1, waiting for transfers between devices: none -> 268 us  [on_device(): pieces = lax.all_gather(partial_value, 'fs')]
    psum x1 -> x0, waiting for transfers between devices: 115 us -> none  [on_device(): summed = lax.psum(partial_value, 'fs')]
    reduce_sum x0 -> x1, other arithmetic: none -> 9.93 us  [on_device(): summed = jnp.sum(pieces, axis=0)]
  transfers between devices with their start and end apart: 4 -> 4, of which waited for: 4 -> 4; matrix products, arithmetic and copies ran while one was open for 3% -> 2% of each run, Pallas kernels for 0% -> 0%
where the time goes in v1:
time: 566 us
  waiting for transfers between devices  466 us (82%)
  blocking collectives  45.4 us (8%)
  local copies, waits for them, and re-layouts  21.4 us (4%)
  between operations  14.6 us (3%)
  other arithmetic  11 us (2%)
  matrix products  7.35 us (1%)
    all_gather x1, waiting for transfers between devices, on_device(): pieces = lax.all_gather(partial_value, 'fs')  268 us
    all_gather x1, waiting for transfers between devices, on_device(): lax.all_gather(half_copy[:, key_cols:], 'fs', axis=0, tiled=True)  86.1 us
    all_gather x1, waiting for transfers between devices, on_device(): lax.all_gather(basis, 'fs', axis=0, tiled=True)  58.5 us
    all_gather x1, waiting for transfers between devices, on_device(): lax.all_gather(half_copy[:, :key_cols], 'fs', axis=0, tiled=True)  52.2 us
    all_gather x1, blocking collectives, on_device(): all_directions = lax.all_gather(direction, 'fs', axis=0, tiled=True)  42.4 us
    unnamed x23, local copies, waits for them, and re-layouts  17.2 us
  transfers between devices with their start and end apart: 4, of which 4 were waited for; matrix products, arithmetic and copies ran while one was open for 2% of the time, Pallas kernels for 0%

profile of v1, /device:TPU:0, one launch (start us, length us, event | category | flops | bytes accessed | tf_op | source)
XLA Modules:
  0.0 565.7 jit_solution(10767465060162287686)
XLA Ops:
  7.2 0.0 all-gather.6.cloned.1.call-start
  7.2 0.7 all-gather.6.cloned.1.call-update
  7.9 0.0 all-gather.12.cloned.1.call-start
  8.0 0.0 copy-start
  8.0 1.4 constant_dynamic-update-slice_fusion.1
  9.4 0.5 copy-done
  9.9 0.2 constant_dynamic-update-slice_fusion
  10.0 58.5 %all-gather.6.cloned.1.call-done = bf16[2048,256]{1,0:T(8,128)(2,1)} async-done(((bf16[128,256]{1,0:T(8,128)(2,1)}), bf16[2048,256]{1,0:T(8,128)(2,1)}) %all-gather.6.cloned.1.call-update) | async-done | bytes 1048592 | tf_op jit(solution)/shard_map/all_gather | solution.py:31
  68.6 3.7 fusion.6
  72.3 1.0 fusion.1
  73.4 0.0 copy-start.2
  73.4 2.2 convolution_add_fusion
  75.5 0.0 all-gather.12.cloned.1.call-update
  75.6 0.0 all-gather.8.cloned.1.call-start
  75.6 1.2 copy.21
  76.9 0.0 copy-done.2
  76.9 0.1 copy.20
  77.0 268.1 %all-gather.12.cloned.1.call-done = f32[4096,1536]{1,0:T(8,128)} async-done(((f32[256,1536]{1,0:T(8,128)}), f32[4096,1536]{1,0:T(8,128)}) %all-gather.12.cloned.1.call-update) | async-done | bytes 25165840 | tf_op jit(solution)/shard_map/all_gather | solution.py:42
  345.0 0.0 copy-start.3
  345.1 0.0 copy-start.4
  345.1 9.9 %reduce_sum.18 = f32[256,1536]{1,0:T(8,128)S(1)} reduce(f32[16,256,1536]{2,1,0:T(8,128)} %bitcast.9, f32[]{:T(128)} %constant.3.clone.1), dimensions={0}, to_apply=%region_0.0 | reduce | flops 5898240 | bytes 26738692 | tf_op jit(solution)/shard_map/reduce_sum | solution.py:43
  355.0 1.0 multiply_reduce_fusion
  356.0 3.1 psum.7
  359.8 0.0 copy-done.3
  359.8 0.0 copy-done.4
  359.8 0.0 copy-done.5
  359.8 0.0 copy-done.6
  359.8 0.1 divide_convert_fusion
  359.9 42.4 %all_gather.21 = bf16[256,1536]{1,0:T(8,128)(2,1)S(1)} all-gather(bf16[16,1536]{1,0:T(8,128)(2,1)S(1)} %get-tuple-element.22), channel_id=1, replica_groups=mesh['fs'=16,'tp'=2] {'fs'}, dimensions={0}, use_global_device_ids=true | all-gather | bytes 835584 | tf_op jit(solution)/shard_map/all_gather | solution.py:54
  402.3 0.0 copy-done.1
  402.3 0.4 fusion.4
  402.7 0.7 slice.44
  403.4 0.0 all-gather.8.cloned.1.call-update
  403.4 0.0 all-gather.10.cloned.1.call-start
  403.4 0.7 slice.45
  404.1 0.0 all-gather.10.cloned.1.call-update
  404.3 0.6 slice.48
  404.9 0.6 slice.46
  405.6 0.6 slice.49
  406.2 0.6 slice.47
  406.8 1.0 copy.23
  407.8 1.0 copy.25
  408.8 0.8 copy.22
  409.6 0.8 copy.24
  410.5 52.2 %all-gather.8.cloned.1.call-done = bf16[2048,512]{0,1:T(8,128)(2,1)} async-done(((bf16[128,512]{0,1:T(8,128)(2,1)}), bf16[2048,512]{0,1:T(8,128)(2,1)}) %all-gather.8.cloned.1.call-update) | async-done | bytes 2097168 | tf_op jit(solution)/shard_map/all_gather | solution.py:60
  462.7 3.9 copy.26
  466.6 86.1 %all-gather.10.cloned.1.call-done = bf16[2048,1024]{0,1:T(8,128)(2,1)} async-done(((bf16[128,1024]{0,1:T(8,128)(2,1)}), bf16[2048,1024]{0,1:T(8,128)(2,1)}) %all-gather.10.cloned.1.call-update) | async-done | bytes 4194320 | tf_op jit(solution)/shard_map/all_gather | solution.py:61
  552.7 6.4 %copy.27 = bf16[2048,1024]{1,0:T(8,128)(2,1)} copy(bf16[2048,1024]{0,1:T(8,128)(2,1)} %all-gather.10.cloned.1.call-done) | data formatting | bytes 8388608
  (7 shorter events, 0.1 us)
Async XLA Ops:
  7.2 61.4 %all-gather.6.cloned.1.call-start = ((), (), s32[]{:S(2)}) async-start(), calls=%async_computation | async-start | bytes 1114112 | tf_op jit(solution)/shard_map/all_gather | solution.py:31
  7.9 337.1 %all-gather.12.cloned.1.call-start = ((), (), s32[]{:S(2)}) async-start(), calls=%async_computation.3 | async-start | bytes 26738688 | tf_op jit(solution)/shard_map/all_gather | solution.py:42
  8.0 1.9 copy-start
  73.4 3.5 copy-start.2
  75.6 387.1 %all-gather.8.cloned.1.call-start = ((), (), s32[]{:S(2)}) async-start(), calls=%async_computation.1 | async-start | bytes 2228224 | tf_op jit(solution)/shard_map/all_gather | solution.py:60
  345.0 14.7 %copy-start.3 = (f32[16,1024]{1,0:T(8,128)S(1)}, f32[16,1024]{1,0:T(8,128)}, u32[]{:S(2)}) copy-start(f32[16,1024]{1,0:T(8,128)} %param.19) | copy-start | bytes 196612
  345.1 14.7 %copy-start.4 = (f32[16,1024]{1,0:T(8,128)S(1)}, f32[16,1024]{1,0:T(8,128)}, u32[]{:S(2)}) copy-start(f32[16,1024]{1,0:T(8,128)} %param.18) | copy-start | bytes 196612
  345.1 14.7 %copy-start.5 = (f32[16,512]{1,0:T(8,128)S(1)}, f32[16,512]{1,0:T(8,128)}, u32[]{:S(2)}) copy-start(f32[16,512]{1,0:T(8,128)} %param.17) | copy-start | bytes 98308
  345.1 14.8 %copy-start.6 = (f32[16,512]{1,0:T(8,128)S(1)}, f32[16,512]{1,0:T(8,128)}, u32[]{:S(2)}) copy-start(f32[16,512]{1,0:T(8,128)} %param.16) | copy-start | bytes 98308
  345.1 57.2 %copy-start.1 = (bf16[128,256]{1,0:T(8,128)(2,1)S(1)}, bf16[128,256]{1,0:T(8,128)(2,1)}, u32[]{:S(2)}) copy-start(bf16[128,256]{1,0:T(8,128)(2,1)} %param.13) | copy-start | bytes 196612
  403.4 149.4 %all-gather.10.cloned.1.call-start = ((), (), s32[]{:S(2)}) async-start(), calls=%async_computation.2 | async-start | bytes 4456448 | tf_op jit(solution)/shard_map/all_gather | solution.py:61
Sparse Core Ops, SparseCore 0:
  10.7 57.7 all-gather.5
  75.7 269.3 all-gather.11
  403.5 59.1 all-gather.7
  465.8 86.8 all-gather.9
